TPU v7x, 128 devices: a whole 4x4x4 slice. The times are simulated.
128 devices in a mesh: ep: 32 (over z, y, core), tp: 4 (over x).
Axes of the slice: x: 4, y: 4, z: 4, core: 2. Of those that a mesh axis runs over, the one named last changes fastest.
Arguments:
- queries: bfloat16 [32768, 1024], P('ep', 'tp'), may hold values from -6 to 6
- keys: bfloat16 [32768, 1024], P('ep', 'tp'), may hold values from -6 to 6
- values: bfloat16 [32768, 2048], P('ep', 'tp'), may hold values from -6 to 6
- log_input_gate: float32 [32768, 8], P('ep', 'tp'), may hold values from -6 to 103
- forget_preactivation: float32 [32768, 8], P('ep', 'tp'), may hold values from 0 to 16
- forget_offset: float32 [32768, 8], P('ep', 'tp'), may hold values from -0.7 to 0
- head_norm_scale: float32 [2048], P('tp'), may hold values from 0.1 to 1.9
- memory_output_weight: bfloat16 [2048, 4096], P('tp'), may hold values from -0.125 to 0.125
- second_micro_tokens: bfloat16 [16384, 4096], P('ep'), may hold values from -6 to 6
- expert_norm_scale: float32 [4096], replicated, may hold values from 0.1 to 1.9
- expert_choice_index: int32 [16384, 2], P('ep'), may hold values from 0 to 63, all different within a row; in each aligned block of 512 rows (0 to 511, 512 to 1023, ...) at most 24 rows name the same one
- group_likelihood: float32 [16384], P('ep'), may hold values from 0.2 to 1
- expert_raw_weight: float32 [16384, 2], P('ep'), may hold values from 0.1 to 1
- gate_weight: bfloat16 [64, 4096, 1024], P('ep', None, 'tp'), may hold values from -0.09375 to 0.09375
- up_weight: bfloat16 [64, 4096, 1024], P('ep', None, 'tp'), may hold values from -0.09375 to 0.09375
- down_weight: bfloat16 [64, 1024, 4096], P('ep', 'tp'), may hold values from -0.1875 to 0.1875
Outputs:
- mixed: bfloat16 [32768, 4096], P(('ep', 'tp'))
- routed: bfloat16 [16384, 4096], P('ep', 'tp')
Inputs may be any that keep to these rules, and one draw needn't show every extreme that they name: `expert_choice_index`: each row names 2 different experts. Within the 512 rows of one index of ep (aligned blocks) no expert is named more than 24 times, and in some blocks one expert is named exactly 24 times.
All inputs are finite; a program needn't handle non-finite values.
Results may differ from a plain program's by a relative error of at most 0.012.
Values may be sent and summed in bfloat16 or wider, within the bound.
No kernel may reach another device: no remote copies, remote signals or barrier semaphores. Data moves between devices by JAX's collectives and lax.ppermute only.
A program may use at most 192 MiB of HBM per device.

v0:
```python
import math
import jax
import jax.numpy as jnp
from jax import lax
from jax.sharding import Mesh
from jax.sharding import PartitionSpec as P

BLOCK = 128
EP = ("ep_0", "ep_1", "ep_2")
EP_TP = ("ep_0", "ep_1", "ep_2", "tp")
EPSILON = 1e-06
FLOOR_LOG = -1e30


def filled_with(value, identity):
    return jax.tree.map(
        lambda a, e: jnp.broadcast_to(jnp.asarray(e, a.dtype), a.shape), value, identity
    )


def collected_together(value, axis):
    leaves = jax.tree.leaves(value)
    order = sorted(range(len(leaves)), key=lambda k: -leaves[k].size)
    width = (1, *leaves[order[0]].shape)[-1]
    lines = [
        jnp.pad(leaves[k].reshape(-1), (0, -leaves[k].size % width)).reshape(-1, width)
        for k in order
    ]
    both, at, found = (lax.all_gather(jnp.concatenate(lines), axis), 0, {})
    for k, line in zip(order, lines):
        share = both[:, at : at + len(line)].reshape(len(both), -1)
        found[k] = share[:, : leaves[k].size].reshape(-1, *leaves[k].shape)
        at += len(line)
    numbers = iter(range(len(leaves)))
    return jax.tree.map(lambda _: found[next(numbers)], value)


def entering(value, axes, combine, identity):
    before = start = filled_with(value, identity)
    subtotal = value
    for axis in reversed(axes):
        peers, position = (lax.axis_size(axis), lax.axis_index(axis))
        pieces = collected_together(subtotal, axis)
        inside, subtotal = (start, start)
        for k in range(peers):
            passed = k < position
            subtotal = combine(subtotal, jax.tree.map(lambda part: part[k], pieces))
            inside = jax.tree.map(lambda new, old: jnp.where(passed, new, old), subtotal, inside)
        before = combine(inside, before)
    return before


def merge_states(earlier, later):
    memory_one, stable_one, total_one = earlier
    memory_two, stable_two, total_two = later
    highest = jnp.maximum(total_two + stable_one, stable_two)
    weight_one = jnp.exp(total_two + stable_one - highest)
    weight_two = jnp.exp(stable_two - highest)
    memory = weight_one[..., None, None] * memory_one + weight_two[..., None, None] * memory_two
    return (memory, highest, total_one + total_two)


def advance(carry, piece):
    return (merge_states(carry, piece), carry)


def recurrence_portion(
    queries,
    keys,
    values,
    log_input_gate,
    forget_preactivation,
    forget_offset,
    head_norm_scale,
    memory_output_weight,
):
    row_count, head_count = log_input_gate.shape
    key_width = queries.shape[1] // head_count
    value_width = values.shape[1] // head_count
    block_count = row_count // BLOCK
    qk_scale = 1.0 / math.sqrt(key_width)
    query_blocks = queries.reshape(block_count, BLOCK, head_count, key_width)
    key_blocks = keys.reshape(block_count, BLOCK, head_count, key_width)
    value_blocks = values.reshape(block_count, BLOCK, head_count, value_width)
    key_float = key_blocks.astype(jnp.float32) * qk_scale
    forget_log_factor = jax.nn.log_sigmoid(forget_preactivation) + forget_offset
    forget_log_factor = forget_log_factor.reshape(block_count, BLOCK, head_count).transpose(0, 2, 1)
    in_gate = log_input_gate.reshape(block_count, BLOCK, head_count).transpose(0, 2, 1)
    running = jnp.cumsum(forget_log_factor, axis=-1)
    totals = running[..., -1]
    to_end = totals[..., None] - running + in_gate
    block_peak = jnp.max(to_end, axis=-1)
    key_weight = jnp.exp(to_end - block_peak[..., None])
    weighted_keys = (key_float * key_weight.transpose(0, 2, 1)[..., None]).astype(jnp.bfloat16)
    block_memory = jnp.einsum(
        "bshd,bshe->bhde", weighted_keys, value_blocks, preferred_element_type=jnp.float32
    )
    empty = (
        jnp.zeros((head_count, key_width, value_width), jnp.float32),
        jnp.full((head_count,), FLOOR_LOG, jnp.float32),
        jnp.zeros((head_count,), jnp.float32),
    )
    device_state, starts = lax.scan(advance, empty, (block_memory, block_peak, totals))
    incoming = entering(device_state, EP, merge_states, empty)
    memory, peak, unused = merge_states(incoming, starts)
    scores = (
        jnp.einsum("bthd,bshd->bhts", query_blocks, key_blocks, preferred_element_type=jnp.float32)
        * qk_scale
    )
    causal = jnp.tril(jnp.ones((BLOCK, BLOCK), dtype=bool))
    log_weight = running[..., :, None] - running[..., None, :] + in_gate[..., None, :]
    log_weight = jnp.where(causal, log_weight, -jnp.inf)
    carried = running + peak[..., None]
    stable = jnp.maximum(carried, jnp.max(log_weight, axis=-1))
    inner = (scores * jnp.exp(log_weight - stable[..., None])).astype(jnp.bfloat16)
    outer = jnp.exp(carried - stable)
    memory_half = memory.astype(jnp.bfloat16)
    state = outer[..., None] * jnp.einsum(
        "bthd,bhde->bhte", query_blocks, memory_half, preferred_element_type=jnp.float32
    )
    state = state + jnp.einsum(
        "bhts,bshe->bhte", inner, value_blocks, preferred_element_type=jnp.float32
    )
    state = state * lax.rsqrt(jnp.mean(state * state, axis=-1, keepdims=True) + EPSILON)
    hidden = state.transpose(0, 2, 1, 3).reshape(row_count, head_count * value_width)
    hidden = (hidden * head_norm_scale).astype(jnp.bfloat16)
    return lax.psum_scatter(
        jnp.dot(hidden, memory_output_weight, preferred_element_type=jnp.float32).astype(
            jnp.bfloat16
        ),
        "tp",
        scatter_dimension=0,
        tiled=True,
    )


def expert_half(
    second_micro_tokens,
    expert_norm_scale,
    expert_choice_index,
    group_likelihood,
    expert_raw_weight,
    gate_weight,
    up_weight,
    down_weight,
):
    token_count, model_width = second_micro_tokens.shape
    pick_count = expert_choice_index.shape[1]
    local_experts = gate_weight.shape[0]
    ep_size = lax.axis_size(EP)
    tp_size = lax.axis_size("tp")
    expert_count = local_experts * ep_size
    capacity = tp_size * max(1, 3 * pick_count * token_count // (2 * expert_count * tp_size))
    token_float = second_micro_tokens.astype(jnp.float32)
    normed = token_float * lax.rsqrt(
        jnp.mean(token_float * token_float, axis=-1, keepdims=True) + EPSILON
    )
    normed = (normed * expert_norm_scale).astype(jnp.bfloat16)
    share = expert_raw_weight / jnp.sum(expert_raw_weight, axis=1, keepdims=True)
    route_weight = group_likelihood[:, None] * share
    flat_expert = expert_choice_index.reshape(-1)
    one_hot = (flat_expert[:, None] == jnp.arange(expert_count, dtype=jnp.int32)[None, :]).astype(
        jnp.int32
    )
    slot_rank = jnp.sum(jnp.cumsum(one_hot, axis=0) * one_hot, axis=1) - 1
    owner = flat_expert // local_experts
    local_index = flat_expert % local_experts
    slot_index = owner * (local_experts * capacity) + local_index * capacity + slot_rank
    slot_total = local_experts * ep_size * capacity
    token_index = jnp.arange(token_count * pick_count, dtype=jnp.int32) // pick_count
    slot_token = jnp.zeros((slot_total,), jnp.int32).at[slot_index].set(token_index)
    slot_used = jnp.zeros((slot_total,), bool).at[slot_index].set(True)
    outgoing = jnp.where(slot_used[:, None], normed[slot_token], jnp.zeros((), jnp.bfloat16))
    outgoing = outgoing.reshape(ep_size, local_experts, capacity, model_width)
    arrived = lax.all_to_all(outgoing, EP, split_axis=0, concat_axis=0, tiled=True)
    gate = jnp.einsum("serd,edf->serf", arrived, gate_weight, preferred_element_type=jnp.float32)
    upward = jnp.einsum("serd,edf->serf", arrived, up_weight, preferred_element_type=jnp.float32)
    hidden = (jax.nn.silu(gate) * upward).astype(jnp.bfloat16)
    unit_width = down_weight.shape[1]
    own_columns = lax.all_to_all(down_weight, "tp", split_axis=2, concat_axis=1, tiled=True)
    column_count = own_columns.shape[2]
    zero_total = jnp.zeros((column_count, ep_size, local_experts, capacity), jnp.float32)
    total = zero_total
    piece = lax.all_gather(hidden, "tp", axis=3, tiled=True)
    for group in range(piece.shape[3] // unit_width):
        group_units = piece[:, :, :, group * unit_width : (group + 1) * unit_width]
        down_rows = lax.dynamic_slice_in_dim(own_columns, group * unit_width, unit_width, 1)
        partial_value = jnp.einsum(
            "serf,efc->cser", group_units, down_rows, preferred_element_type=jnp.float32
        ).astype(jnp.bfloat16)
        total = total + lax.optimization_barrier(partial_value).astype(jnp.float32)
    finished = total.astype(jnp.bfloat16)
    returned = lax.all_to_all(finished, EP, split_axis=1, concat_axis=1, tiled=True)
    flat_result = returned.reshape(returned.shape[0], slot_total)
    picked = jnp.take(flat_result, slot_index, axis=1).astype(jnp.float32)
    picked = picked.reshape(flat_result.shape[0], token_count, pick_count)
    combined = jnp.sum(picked * route_weight[None], axis=2)
    return combined.T.astype(jnp.bfloat16)


def per_device(
    queries,
    keys,
    values,
    log_input_gate,
    forget_preactivation,
    forget_offset,
    head_norm_scale,
    memory_output_weight,
    second_micro_tokens,
    expert_norm_scale,
    expert_choice_index,
    group_likelihood,
    expert_raw_weight,
    gate_weight,
    up_weight,
    down_weight,
):
    mixed = recurrence_portion(
        queries,
        keys,
        values,
        log_input_gate,
        forget_preactivation,
        forget_offset,
        head_norm_scale,
        memory_output_weight,
    )
    routed = expert_half(
        second_micro_tokens,
        expert_norm_scale,
        expert_choice_index,
        group_likelihood,
        expert_raw_weight,
        gate_weight,
        up_weight,
        down_weight,
    )
    return (mixed, routed)


def solution(mesh):
    split = Mesh(mesh.devices.reshape(4, 4, 2, mesh.shape["tp"]), ("ep_0", "ep_1", "ep_2", "tp"))
    placed = (
        P(EP, "tp"),
        P(EP, "tp"),
        P(EP, "tp"),
        P(EP, "tp"),
        P(EP, "tp"),
        P(EP, "tp"),
        P("tp"),
        P("tp", None),
        P(EP, None),
        P(),
        P(EP, None),
        P(EP),
        P(EP, None),
        P(EP, None, "tp"),
        P(EP, None, "tp"),
        P(EP, "tp", None),
    )
    return jax.shard_map(
        per_device,
        mesh=split,
        in_specs=placed,
        out_specs=(P(EP_TP, None), P(EP, "tp")),
        check_vma=False,
    )
```

profile of v0, /device:TPU:2, one launch (start us, length us, event | category | flops | bytes accessed | tf_op | source)
XLA Modules:
  0.0 469.7 jit_solution(17323385805331098350)
XLA Ops:
  9.4 18.0 %reduce-window.6 = s32[64,8,128]{2,1,0:T(8,128)S(1)} reduce-window(s32[64,8,128]{2,1,0:T(8,128)S(1)} %fusion.71, s32[]{:T(128)} %constant.116.clone.1), window={size=1x1x128 pad=0_0x0_0x127_0}, to_apply=%region_7.8 | reduce-window | flops 8323072 | bytes 524292 | tf_op jit(solution)/shard_map/reduce-window
  28.1 4.3 scatter_custom_fusion.1
  32.4 3.1 fusion.12
  35.5 4.6 scatter_custom_fusion
  40.3 5.8 %fusion.14 = bf16[512,4096]{1,0:T(8,128)(2,1)} fusion(bf16[512,4096]{1,0:T(8,128)(2,1)} %param.26, f32[4096]{0:T(1024)S(1)} %copy-done.10, f32[512]{0:T(512)S(1)} %add_rsqrt_fusion), kind=kLoop, calls=%fused_computation.29 | loop fusion | flops 8388608 | bytes 8407040 | tf_op jit(solution)/shard_map/convert_element_type | solution.py:158
  46.1 24.8 %gather_fusion = bf16[1536,4096]{1,0:T(8,128)(2,1)} fusion(bf16[512,4096]{1,0:T(8,128)(2,1)} %fusion.14, s32[2048]{0:T(1024)S(1)} %pad_clamp_fusion), kind=kCustom, calls=%fused_computation | custom fusion | bytes 25171968 | tf_op jit(solution)/shard_map/gather | solution.py:173
  70.9 10.7 %broadcast_select_fusion.2 = bf16[32,2,24,4096]{3,2,1,0:T(8,128)(2,1)} fusion(bf16[32,2,24,4096]{3,2,1,0:T(8,128)(2,1)} %bitcast.456, pred[32,2,24]{2,1,0:T(4,128)(4,1)S(1)} %broadcast_in_dim.57), kind=kLoop, calls=%fused_computation.20 | loop fusion | flops 6291456 | bytes 25167360 | tf_op jit(solution)/shard_map/jit(_where)/select_n | solution.py:173
  81.6 8.6 %all-to-all-start = ((bf16[32,2,24,4096]{3,2,1,0:T(8,128)(2,1)}), bf16[32,2,24,4096]{3,2,1,0:T(8,128)(2,1)}, u32[]{:S(2)}, u32[]{:S(2)}) async-start(bf16[32,2,24,4096]{3,2,1,0:T(8,128)(2,1)} %broadcast_select_fusion.2), calls=%async_computation.1 | async-start | bytes 25165824 | tf_op jit(solution)/shard_map/all_to_all | solution.py:175
  94.4 7.8 %while.21 = (s32[]{:T(128)}, f32[2,128,256]{2,1,0:T(8,128)S(1)}, f32[2]{0:T(128)S(1)}, f32[2]{0:T(128)S(1)}, f32[8,2,128,256]{3,2,1,0:T(8,128)}, /*index=5*/f32[...) while((s32[]{:T(128)}, f32[2,128,256]{2,1,0:T(8,128)S(1)}, ...), condition=%wide.region_3.4_spmd.clone, body=%wide.region_2.3_spmd.clone.sunk | while | flops 327699 | bytes 1311534 | solution.py:103
  102.3 2.2 all-gather.3
  105.9 42.7 %all-gather.12.cloned.1.call-done = f32[4,258,256]{2,1,0:T(8,128)} async-done(((f32[1,258,256]{2,1,0:T(8,128)}), f32[4,258,256]{2,1,0:T(8,128)}) %all-gather.12.cloned.1.call-update) | async-done | bytes 1056784 | tf_op jit(solution)/shard_map/all_gather | solution.py:29
  153.0 2.0 reshape.1120
  157.4 79.3 %all-gather.14.cloned.1.call-done = f32[4,258,256]{2,1,0:T(8,128)} async-done(((f32[1,258,256]{2,1,0:T(8,128)}), f32[4,258,256]{2,1,0:T(8,128)}) %all-gather.14.cloned.1.call-update) | async-done | bytes 1056784 | tf_op jit(solution)/shard_map/all_gather | solution.py:29
  237.5 19.7 %all-to-all-done = bf16[32,2,24,4096]{3,2,1,0:T(8,128)(2,1)} async-done(((bf16[32,2,24,4096]{3,2,1,0:T(8,128)(2,1)}), bf16[32,2,24,4096]{3,2,1,0:T(8,128)(2,1)}, u32[]{:S(2)}, u32[]{:S(2)}) %all-to-all-start) | async-done | bytes 12582944 | tf_op jit(solution)/shard_map/all_to_all | solution.py:175
  257.2 7.6 %fusion.10 = f32[2,32,24,256]{3,2,1,0:T(8,128)S(1)} fusion(bf16[32,2,24,4096]{3,2,1,0:T(8,128)(2,1)} %all-to-all-done, bf16[2,4096,256]{2,1,0:T(8,128)(2,1)} %param.31), kind=kOutput, calls=%fused_computation.23 | convolution fusion | flops 3221225472 | bytes 18350080 | tf_op jit(solution)/shard_map/serd,edf->serf/dot_general | solution.py:176
  264.8 10.3 %fusion.21 = bf16[32,2,24,256]{3,2,0,1:T(8,128)(2,1)} fusion(f32[2,32,24,256]{3,2,1,0:T(8,128)S(1)} %fusion.10, bf16[2,4096,256]{2,1,0:T(8,128)(2,1)} %param.32, bf16[32,2,24,4096]{3,2,1,0:T(8,128)(2,1)} %all-to-all-done), kind=kOutput, calls=%fused_computation.50 | convolution fusion | flops 3223584768 | bytes 19136512 | tf_op jit(solution)/shard_map/serd,edf->serf/dot_general | solution.py:177
  277.7 2.3 fusion.32
  280.0 3.7 fusion.19
  283.8 2.0 fusion.20
  288.0 7.5 %convolution_convert_fusion = bf16[1024,4096]{1,0:T(8,128)(2,1)} fusion(bf16[512,4096]{1,0:T(8,128)(2,1)S(1)} %copy-done.16, f32[64,8,8,128]{3,2,1,0:T(8,128)S(1)} %bitcast.464, f32[512]{0:T(512)S(1)} %copy-done.17), kind=kOutput, calls=%fused_computation.30 | convolution fusion | flops 4300210176 | bytes 14682112 | tf_op jit(solution)/shard_map/dot_general | solution.py:128
  295.6 11.1 %copy.166 = bf16[2,256,4096]{1,0,2:T(2,128)(2,1)} copy(bf16[2,256,4096]{2,1,0:T(8,128)(2,1)} %param.33) | data formatting | bytes 8388608 | tf_op args[15]
  306.7 67.7 %all_to_all.28 = bf16[2,256,4096]{1,0,2:T(2,128)(2,1)} all-to-all(bf16[2,256,4096]{1,0,2:T(2,128)(2,1)} %copy.166), channel_id=1, replica_groups=mesh['ep_0'=4,'ep_1'=4,'ep_2'=2,'tp'=4] {'tp'}, dimensions={2} | all-to-all | bytes 8388608 | tf_op jit(solution)/shard_map/all_to_all | solution.py:180
  374.4 11.3 %copy.167 = bf16[2,256,4,1024]{3,1,2,0:T(8,128)(2,1)} copy(bf16[2,256,4,1024]{1,0,3,2:T(2,128)(2,1)} %bitcast.462) | data formatting | bytes 8388608 | tf_op jit(solution)/shard_map/all_to_all | solution.py:180
  385.7 2.6 convert_bitcast_fusion.3
  388.7 2.3 convert_bitcast_fusion.2
  393.0 3.2 add_convert_fusion
  396.3 2.0 copy.168
  398.3 4.2 all-to-all-start.2
  403.3 41.2 %all-to-all-done.2 = bf16[1024,32,2,24]{0,3,2,1:T(8,128)(2,1)S(1)} async-done(((bf16[1024,32,2,24]{0,3,2,1:T(8,128)(2,1)}), bf16[1024,32,2,24]{0,3,2,1:T(8,128)(2,1)S(1)}, u32[]{:S(2)}, u32[]{:S(2)}) %all-to-all-start.2) | async-done | bytes 3145760 | tf_op jit(solution)/shard_map/all_to_all | solution.py:193
  444.5 5.4 %gather_fusion.1 = bf16[1024,1024]{1,0:T(8,128)(2,1)} fusion(bf16[1024,1536]{0,1:T(8,128)(2,1)S(1)} %bitcast.455, s32[1024]{0:T(1024)S(1)} %broadcast_clamp_fusion), kind=kCustom, calls=%fused_computation.1 | custom fusion | bytes 4198400 | tf_op jit(solution)/shard_map/jit(_take)/gather | solution.py:195
  449.9 2.7 gather.14
  452.6 9.4 %multiply_reduce_fusion = bf16[1024,512]{0,1:T(8,128)(2,1)} fusion(bf16[1024,512,2]{0,2,1:T(2,128)(2,1)S(1)} %gather.14, pred[512,2]{1,0:T(8,128)(4,1)S(1)} %copy.162, f32[512,2]{1,0:T(8,128)S(1)} %copy.169), kind=kLoop, calls=%fused_computation.34 | loop fusion | flops 3670016 | bytes 3150848 | tf_op jit(solution)/shard_map/reduce_sum | solution.py:197
  (210 shorter events, 30.5 us)
Async XLA Ops:
  9.4 30.9 %copy-start.10 = (f32[4096]{0:T(1024)S(1)}, f32[4096]{0:T(1024)}, u32[]{:S(2)}) copy-start(f32[4096]{0:T(1024)} %param.27) | copy-start | bytes 49156
  81.5 8.7 %copy-start.13 = (f32[1024,2]{0,1:T(2,128)S(1)}, f32[1024,2]{0,1:T(2,128)}, u32[]{:S(2)}) copy-start(f32[1024,2]{0,1:T(2,128)} %param.23) | copy-start | bytes 24580
  81.5 8.7 %copy-start.14 = (f32[1024,2]{0,1:T(2,128)S(1)}, f32[1024,2]{0,1:T(2,128)}, u32[]{:S(2)}) copy-start(f32[1024,2]{0,1:T(2,128)} %param.22) | copy-start | bytes 24580
  81.5 9.5 %copy-start.9 = (f32[1024,2]{0,1:T(2,128)S(1)}, f32[1024,2]{0,1:T(2,128)}, u32[]{:S(2)}) copy-start(f32[1024,2]{0,1:T(2,128)} %param.21) | copy-start | bytes 24580
  81.6 9.9 %copy-start.8 = (bf16[1024,256]{1,0:T(8,128)(2,1)S(1)}, bf16[1024,256]{1,0:T(8,128)(2,1)}, u32[]{:S(2)}) copy-start(bf16[1024,256]{1,0:T(8,128)(2,1)} %param.19) | copy-start | bytes 1572868
  81.6 11.1 %copy-start.3 = (bf16[1024,512]{1,0:T(8,128)(2,1)S(1)}, bf16[1024,512]{1,0:T(8,128)(2,1)}, u32[]{:S(2)}) copy-start(bf16[1024,512]{1,0:T(8,128)(2,1)} %param.20) | copy-start | bytes 3145732
  81.6 175.6 %all-to-all-start = ((bf16[32,2,24,4096]{3,2,1,0:T(8,128)(2,1)}), bf16[32,2,24,4096]{3,2,1,0:T(8,128)(2,1)}, u32[]{:S(2)}, u32[]{:S(2)}) async-start(bf16[32,2,24,4096]{3,2,1,0:T(8,128)(2,1)} %broadcast_select_fusion.2), calls=%async_computation.1 | async-start | bytes 25165824 | tf_op jit(solution)/shard_map/all_to_all | solution.py:175
  90.2 58.4 %all-gather.12.cloned.1.call-start = ((), (), s32[]{:S(2)}) async-start(), calls=%async_computation.6 | async-start | bytes 1351680 | tf_op jit(solution)/shard_map/all_gather | solution.py:29
  105.8 130.8 %all-gather.14.cloned.1.call-start = ((), (), s32[]{:S(2)}) async-start(), calls=%async_computation.7 | async-start | bytes 1351680 | tf_op jit(solution)/shard_map/all_gather | solution.py:29
  148.6 7.9 %copy-start.1 = (f32[4,258,256]{2,1,0:T(8,128)S(1)}, f32[4,258,256]{2,1,0:T(8,128)}, u32[]{:S(2)}) copy-start(f32[4,258,256]{2,1,0:T(8,128)} %all-gather.12.cloned.1.call-done) | copy-start | bytes 3170308
  152.4 233.3 %all-gather.10.cloned.1.call-start = ((), (), s32[]{:S(2)}) async-start(), calls=%async_computation.5 | async-start | bytes 3932160 | tf_op jit(solution)/shard_map/all_gather | solution.py:184
  275.1 1.9 copy-start.4
  275.1 2.0 copy-start.5
  275.1 2.0 copy-start.6
  275.2 2.0 copy-start.7
  275.2 186.9 %reduce-scatter.2.cloned.1.call-start = ((), (), s32[]{:S(2)}) async-start(), calls=%async_computation.4 | async-start | bytes 10485760 | tf_op jit(solution)/shard_map/reduce_scatter | solution.py:127
  283.7 3.2 copy-start.17
  285.7 2.2 copy-start.16
  385.7 3.0 copy-start
  388.7 2.3 copy-start.2
  398.3 4.5 copy-start.11
  398.3 4.8 %copy-start.12 = (f32[512,2]{0,1:T(2,128)S(1)}, f32[512,2]{0,1:T(2,128)}, u32[]{:S(2)}) copy-start(f32[512,2]{0,1:T(2,128)} %param.30) | copy-start | bytes 12292
  398.3 4.8 %copy-start.15 = (f32[512]{0:T(512)S(1)}, f32[512]{0:T(512)}, u32[]{:S(2)}) copy-start(f32[512]{0:T(512)} %param.29) | copy-start | bytes 6148
  398.3 46.2 %all-to-all-start.2 = ((bf16[1024,32,2,24]{0,3,2,1:T(8,128)(2,1)}), bf16[1024,32,2,24]{0,3,2,1:T(8,128)(2,1)S(1)}, u32[]{:S(2)}, u32[]{:S(2)}) async-start(bf16[1024,32,2,24]{0,3,2,1:T(8,128)(2,1)} %copy.168), calls=%async_computation.3 | async-start | bytes 6291456 | tf_op jit(solution)/shard_map/all_to_all | solution.py:193
Sparse Core Ops, SparseCore 0:
  105.9 42.5 all-gather.11
  152.5 84.0 all-gather.13
Sparse Core Ops, SparseCore 1:
  275.3 48.7 all-gather.9
  326.9 99.7 reduce-scatter.1
where the time goes:
time: 477 us; the launch traced here: 470 us
  waiting for transfers between devices  183 us (38%)
  local copies, waits for them, and re-layouts  81.5 us (17%)
  blocking collectives  69.9 us (15%)
  other arithmetic  65.1 us (14%)
  matrix products  39.9 us (8%)
  between operations  16.4 us (3%)
  starting transfers between devices  13.7 us (3%)
    all_gather x2, waiting for transfers between devices, collected_together(): both, at, found = (lax.all_gather(jnp.concatenate(lines), axis), 0, {})  122 us
    all_to_all x1, blocking collectives, expert_half(): lax.all_to_all(down_weight, 'tp', split_axis=2, concat_axis=1, tiled=True)  67.7 us
    all_to_all x1, waiting for transfers between devices, expert_half(): lax.all_to_all(finished, EP, split_axis=1, concat_axis=1, tiled=True)  41.2 us
    gather x1, local copies, waits for them, and re-layouts, expert_half(): normed[slot_token]  24.8 us
    all_to_all x1, waiting for transfers between devices, expert_half(): lax.all_to_all(outgoing, EP, split_axis=0, concat_axis=0, tiled=True)  19.7 us
    another operation x5, other arithmetic  18.2 us
    unnamed x46, local copies, waits for them, and re-layouts  13.6 us
    all_to_all x1, local copies, waits for them, and re-layouts, expert_half(): lax.all_to_all(down_weight, 'tp', split_axis=2, concat_axis=1, tiled=True)  11.3 us
  transfers between devices with their start and end apart: 6, of which 4 were waited for; matrix products, arithmetic and copies ran while one was open for 20% of the time, Pallas kernels for 0%

commit v1 on v0

--- a/solution.py
+++ b/solution.py
@@ -177,7 +177,10 @@
     upward = jnp.einsum("serd,edf->serf", arrived, up_weight, preferred_element_type=jnp.float32)
     hidden = (jax.nn.silu(gate) * upward).astype(jnp.bfloat16)
     unit_width = down_weight.shape[1]
-    own_columns = lax.all_to_all(down_weight, "tp", split_axis=2, concat_axis=1, tiled=True)
+    peers_2 = lax.axis_size("tp")
+    shards = jnp.stack(jnp.split(down_weight, peers_2, axis=2), axis=0)
+    shards = lax.all_to_all(shards, "tp", split_axis=0, concat_axis=0)
+    own_columns = jnp.concatenate(shards, axis=1)
     column_count = own_columns.shape[2]
     zero_total = jnp.zeros((column_count, ep_size, local_experts, capacity), jnp.float32)
     total = zero_total

time: 477 us -> 457 us (0.958)
  local copies, waits for them, and re-layouts: 81.5 us -> 69.2 us
  blocking collectives: 69.9 us -> 60.7 us
    all_to_all x1 -> x0, local copies, waits for them, and re-layouts: 11.3 us -> none  [expert_half(): lax.all_to_all(down_weight, 'tp', split_axis=2, concat_axis=1, tiled=True)]
    unnamed x46 -> x43, local copies, waits for them, and re-layouts: 13.6 us -> 3.62 us
    all_to_all x1, blocking collectives: 67.7 us -> 58.5 us  [expert_half(): shards = lax.all_to_all(shards, 'tp', split_axis=0, concat_axis=0)]
    another operation x5 -> x6, other arithmetic: 18.2 us -> 18.8 us
  transfers between devices with their start and end apart: 6 -> 6, of which waited for: 4 -> 4; matrix products, arithmetic and copies ran while one was open for 20% -> 17% of each run, Pallas kernels for 0% -> 0%
where the time goes in v1:
time: 457 us; the launch traced here: 449 us
  waiting for transfers between devices  183 us (40%)
  local copies, waits for them, and re-layouts  69.2 us (15%)
  other arithmetic  65.9 us (14%)
  blocking collectives  60.7 us (13%)
  matrix products  36.8 us (8%)
  starting transfers between devices  16.6 us (4%)
  between operations  16.5 us (4%)
    all_gather x2, waiting for transfers between devices, collected_together(): both, at, found = (lax.all_gather(jnp.concatenate(lines), axis), 0, {})  122 us
    all_to_all x1, blocking collectives, expert_half(): shards = lax.all_to_all(shards, 'tp', split_axis=0, concat_axis=0)  58.5 us
    all_to_all x1, waiting for transfers between devices, expert_half(): lax.all_to_all(finished, EP, split_axis=1, concat_axis=1, tiled=True)  41.2 us
    gather x1, local copies, waits for them, and re-layouts, expert_half(): normed[slot_token]  24.8 us
    all_to_all x1, waiting for transfers between devices, expert_half(): lax.all_to_all(outgoing, EP, split_axis=0, concat_axis=0, tiled=True)  19.7 us
    another operation x5, other arithmetic  18.2 us
    select_n x1, other arithmetic, expert_half(): jnp.where(slot_used[:, None], normed[slot_token], jnp.zeros((), jnp.bfloa...  10.6 us
    dot_general x1, matrix products, expert_half(): jnp.einsum('serd,edf->serf', arrived, up_weight, preferred_element_type=j...  10.3 us
  transfers between devices with their start and end apart: 6, of which 4 were waited for; matrix products, arithmetic and copies ran while one was open for 17% of the time, Pallas kernels for 0%

profile of v1, /device:TPU:2, one launch (start us, length us, event | category | flops | bytes accessed | tf_op | source)
XLA Modules:
  0.0 449.4 jit_solution(311819065005290546)
XLA Ops:
  9.4 18.0 %reduce-window.6 = s32[64,8,128]{2,1,0:T(8,128)S(1)} reduce-window(s32[64,8,128]{2,1,0:T(8,128)S(1)} %fusion.71, s32[]{:T(128)} %constant.116.clone.1), window={size=1x1x128 pad=0_0x0_0x127_0}, to_apply=%region_7.8 | reduce-window | flops 8323072 | bytes 524292 | tf_op jit(solution)/shard_map/reduce-window
  28.1 4.3 scatter_custom_fusion.1
  32.4 3.1 fusion.12
  35.5 4.9 %scatter_custom_fusion = pred[1536]{0:T(1024)(128)(4,1)S(1)} fusion(s32[1024]{0:T(1024)S(1)} %bitcast.504, pred[1024]{0:T(1024)(128)(4,1)S(1)} %broadcast.884, pred[]{:T(512)} %constant.134.clone.1), kind=kCustom, calls=%fused_computation.179 | custom fusion | bytes 1537 | tf_op jit(solution)/shard_map/scatter | solution.py:172
  40.5 5.8 %fusion.14 = bf16[512,4096]{1,0:T(8,128)(2,1)} fusion(bf16[512,4096]{1,0:T(8,128)(2,1)} %param.26, f32[4096]{0:T(1024)S(1)} %copy-done.9, f32[512]{0:T(512)S(1)} %add_rsqrt_fusion), kind=kLoop, calls=%fused_computation.29 | loop fusion | flops 8388608 | bytes 8407040 | tf_op jit(solution)/shard_map/convert_element_type | solution.py:158
  46.3 24.8 %gather_fusion = bf16[1536,4096]{1,0:T(8,128)(2,1)} fusion(bf16[512,4096]{1,0:T(8,128)(2,1)} %fusion.14, s32[2048]{0:T(1024)S(1)} %pad_clamp_fusion), kind=kCustom, calls=%fused_computation | custom fusion | bytes 25171968 | tf_op jit(solution)/shard_map/gather | solution.py:173
  71.1 10.6 %broadcast_select_fusion.2 = bf16[32,2,24,4096]{3,2,1,0:T(8,128)(2,1)} fusion(bf16[32,2,24,4096]{3,2,1,0:T(8,128)(2,1)} %bitcast.462, pred[32,2,24]{2,1,0:T(4,128)(4,1)S(1)} %broadcast_in_dim.57), kind=kLoop, calls=%fused_computation.20 | loop fusion | flops 6291456 | bytes 25167360 | tf_op jit(solution)/shard_map/jit(_where)/select_n | solution.py:173
  81.8 8.6 %all-to-all-start.1 = ((bf16[32,2,24,4096]{3,2,1,0:T(8,128)(2,1)}), bf16[32,2,24,4096]{3,2,1,0:T(8,128)(2,1)}, u32[]{:S(2)}, u32[]{:S(2)}) async-start(bf16[32,2,24,4096]{3,2,1,0:T(8,128)(2,1)} %broadcast_select_fusion.2), calls=%async_computation.2 | async-start | bytes 25165824 | tf_op jit(solution)/shard_map/all_to_all | solution.py:175
  94.6 7.8 %while.21 = (s32[]{:T(128)}, f32[2,128,256]{2,1,0:T(8,128)S(1)}, f32[2]{0:T(128)S(1)}, f32[2]{0:T(128)S(1)}, f32[8,2,128,256]{3,2,1,0:T(8,128)}, /*index=5*/f32[...) while((s32[]{:T(128)}, f32[2,128,256]{2,1,0:T(8,128)S(1)}, ...), condition=%wide.region_3.4_spmd.clone, body=%wide.region_2.3_spmd.clone.sunk | while | flops 327699 | bytes 1311534 | solution.py:103
  102.5 2.2 all-gather.3
  106.1 42.7 %all-gather.12.cloned.1.call-done = f32[4,258,256]{2,1,0:T(8,128)} async-done(((f32[1,258,256]{2,1,0:T(8,128)}), f32[4,258,256]{2,1,0:T(8,128)}) %all-gather.12.cloned.1.call-update) | async-done | bytes 1056784 | tf_op jit(solution)/shard_map/all_gather | solution.py:29
  152.8 1.9 reshape.1126
  157.2 79.7 %all-gather.14.cloned.1.call-done = f32[4,258,256]{2,1,0:T(8,128)} async-done(((f32[1,258,256]{2,1,0:T(8,128)}), f32[4,258,256]{2,1,0:T(8,128)}) %all-gather.14.cloned.1.call-update) | async-done | bytes 1056784 | tf_op jit(solution)/shard_map/all_gather | solution.py:29
  237.7 19.7 %all-to-all-done.1 = bf16[32,2,24,4096]{3,2,1,0:T(8,128)(2,1)} async-done(((bf16[32,2,24,4096]{3,2,1,0:T(8,128)(2,1)}), bf16[32,2,24,4096]{3,2,1,0:T(8,128)(2,1)}, u32[]{:S(2)}, u32[]{:S(2)}) %all-to-all-start.1) | async-done | bytes 12582944 | tf_op jit(solution)/shard_map/all_to_all | solution.py:175
  257.4 7.6 %fusion.10 = f32[2,32,24,256]{3,2,1,0:T(8,128)S(1)} fusion(bf16[32,2,24,4096]{3,2,1,0:T(8,128)(2,1)} %all-to-all-done.1, bf16[2,4096,256]{2,1,0:T(8,128)(2,1)} %param.31), kind=kOutput, calls=%fused_computation.23 | convolution fusion | flops 3221225472 | bytes 18350080 | tf_op jit(solution)/shard_map/serd,edf->serf/dot_general | solution.py:176
  265.1 10.3 %fusion.21 = bf16[32,2,24,256]{3,2,0,1:T(8,128)(2,1)} fusion(f32[2,32,24,256]{3,2,1,0:T(8,128)S(1)} %fusion.10, bf16[2,4096,256]{2,1,0:T(8,128)(2,1)} %param.32, bf16[32,2,24,4096]{3,2,1,0:T(8,128)(2,1)} %all-to-all-done.1), kind=kOutput, calls=%fused_computation.51 | convolution fusion | flops 3223584768 | bytes 19136512 | tf_op jit(solution)/shard_map/serd,edf->serf/dot_general | solution.py:177
  277.9 2.3 fusion.32
  280.3 3.7 fusion.19
  284.0 2.0 fusion.20
  288.3 7.4 %convolution_convert_fusion = bf16[1024,4096]{1,0:T(8,128)(2,1)} fusion(bf16[512,4096]{1,0:T(8,128)(2,1)S(1)} %copy-done.15, f32[64,8,8,128]{3,2,1,0:T(8,128)S(1)} %bitcast.470, f32[512]{0:T(512)S(1)} %copy-done.16), kind=kOutput, calls=%fused_computation.30 | convolution fusion | flops 4300210176 | bytes 14682112 | tf_op jit(solution)/shard_map/dot_general | solution.py:128
  295.7 2.7 slice_bitcast_fusion.11
  299.0 58.5 %all_to_all.15 = bf16[4,2,256,1024]{3,2,1,0:T(8,128)(2,1)S(1)} all-to-all(bf16[4,2,256,1024]{3,2,1,0:T(8,128)(2,1)S(1)} %pad_maximum_fusion), channel_id=1, replica_groups=mesh['ep_0'=4,'ep_1'=4,'ep_2'=2,'tp'=4] {'tp'}, dimensions={0} | all-to-all | bytes 8388608 | tf_op jit(solution)/shard_map/all_to_all | solution.py:182
  357.5 2.4 copy.174
  359.9 2.2 fusion.122
  362.2 1.6 copy-done
  367.7 3.4 add_convert_fusion
  371.1 3.4 copy.182
  374.6 7.5 %all-to-all-start.2 = ((bf16[1024,32,2,24]{0,3,2,1:T(8,128)(2,1)}), bf16[1024,32,2,24]{0,3,2,1:T(8,128)(2,1)S(1)}, u32[]{:S(2)}, u32[]{:S(2)}) async-start(bf16[1024,32,2,24]{0,3,2,1:T(8,128)(2,1)} %copy.182), calls=%async_computation.3 | async-start | bytes 6291456 | tf_op jit(solution)/shard_map/all_to_all | solution.py:196
  382.8 41.2 %all-to-all-done.2 = bf16[1024,32,2,24]{0,3,2,1:T(8,128)(2,1)S(1)} async-done(((bf16[1024,32,2,24]{0,3,2,1:T(8,128)(2,1)}), bf16[1024,32,2,24]{0,3,2,1:T(8,128)(2,1)S(1)}, u32[]{:S(2)}, u32[]{:S(2)}) %all-to-all-start.2) | async-done | bytes 3145760 | tf_op jit(solution)/shard_map/all_to_all | solution.py:196
  424.0 5.4 %gather_fusion.1 = bf16[1024,1024]{1,0:T(8,128)(2,1)} fusion(bf16[1024,1536]{0,1:T(8,128)(2,1)S(1)} %bitcast.461, s32[1024]{0:T(1024)S(1)} %broadcast_clamp_fusion), kind=kCustom, calls=%fused_computation.1 | custom fusion | bytes 4198400 | tf_op jit(solution)/shard_map/jit(_take)/gather | solution.py:198
  429.4 2.8 gather.14
  432.2 9.4 %multiply_reduce_fusion = bf16[1024,512]{0,1:T(8,128)(2,1)} fusion(bf16[1024,512,2]{0,2,1:T(2,128)(2,1)S(1)} %gather.14, pred[512,2]{1,0:T(8,128)(4,1)S(1)} %copy.173, f32[512,2]{1,0:T(8,128)S(1)} %copy.183), kind=kLoop, calls=%fused_computation.35 | loop fusion | flops 3670016 | bytes 3150848 | tf_op jit(solution)/shard_map/reduce_sum | solution.py:200
  (210 shorter events, 32.3 us)
Async XLA Ops:
  9.4 31.1 %copy-start.9 = (f32[4096]{0:T(1024)S(1)}, f32[4096]{0:T(1024)}, u32[]{:S(2)}) copy-start(f32[4096]{0:T(1024)} %param.27) | copy-start | bytes 49156
  81.8 8.7 %copy-start.12 = (f32[1024,2]{0,1:T(2,128)S(1)}, f32[1024,2]{0,1:T(2,128)}, u32[]{:S(2)}) copy-start(f32[1024,2]{0,1:T(2,128)} %param.23) | copy-start | bytes 24580
  81.8 8.7 %copy-start.13 = (f32[1024,2]{0,1:T(2,128)S(1)}, f32[1024,2]{0,1:T(2,128)}, u32[]{:S(2)}) copy-start(f32[1024,2]{0,1:T(2,128)} %param.22) | copy-start | bytes 24580
  81.8 9.5 %copy-start.8 = (f32[1024,2]{0,1:T(2,128)S(1)}, f32[1024,2]{0,1:T(2,128)}, u32[]{:S(2)}) copy-start(f32[1024,2]{0,1:T(2,128)} %param.21) | copy-start | bytes 24580
  81.8 9.9 %copy-start.7 = (bf16[1024,256]{1,0:T(8,128)(2,1)S(1)}, bf16[1024,256]{1,0:T(8,128)(2,1)}, u32[]{:S(2)}) copy-start(bf16[1024,256]{1,0:T(8,128)(2,1)} %param.19) | copy-start | bytes 1572868
  81.8 11.1 %copy-start.2 = (bf16[1024,512]{1,0:T(8,128)(2,1)S(1)}, bf16[1024,512]{1,0:T(8,128)(2,1)}, u32[]{:S(2)}) copy-start(bf16[1024,512]{1,0:T(8,128)(2,1)} %param.20) | copy-start | bytes 3145732
  81.8 175.6 %all-to-all-start.1 = ((bf16[32,2,24,4096]{3,2,1,0:T(8,128)(2,1)}), bf16[32,2,24,4096]{3,2,1,0:T(8,128)(2,1)}, u32[]{:S(2)}, u32[]{:S(2)}) async-start(bf16[32,2,24,4096]{3,2,1,0:T(8,128)(2,1)} %broadcast_select_fusion.2), calls=%async_computation.2 | async-start | bytes 25165824 | tf_op jit(solution)/shard_map/all_to_all | solution.py:175
  90.4 58.4 %all-gather.12.cloned.1.call-start = ((), (), s32[]{:S(2)}) async-start(), calls=%async_computation.6 | async-start | bytes 1351680 | tf_op jit(solution)/shard_map/all_gather | solution.py:29
  106.0 130.8 %all-gather.14.cloned.1.call-start = ((), (), s32[]{:S(2)}) async-start(), calls=%async_computation.7 | async-start | bytes 1351680 | tf_op jit(solution)/shard_map/all_gather | solution.py:29
  148.7 7.5 %copy-start.1 = (f32[4,258,256]{2,1,0:T(8,128)S(1)}, f32[4,258,256]{2,1,0:T(8,128)}, u32[]{:S(2)}) copy-start(f32[4,258,256]{2,1,0:T(8,128)} %all-gather.12.cloned.1.call-done) | copy-start | bytes 3170308
  152.6 207.4 %all-gather.10.cloned.1.call-start = ((), (), s32[]{:S(2)}) async-start(), calls=%async_computation.5 | async-start | bytes 3932160 | tf_op jit(solution)/shard_map/all_gather | solution.py:187
  275.4 2.0 copy-start.3
  275.4 2.0 copy-start.4
  275.4 2.0 copy-start.5
  275.4 2.0 copy-start.6
  275.4 166.2 %reduce-scatter.2.cloned.1.call-start = ((), (), s32[]{:S(2)}) async-start(), calls=%async_computation.4 | async-start | bytes 10485760 | tf_op jit(solution)/shard_map/reduce_scatter | solution.py:127
  284.0 3.2 copy-start.16
  286.0 2.2 copy-start.15
  359.9 3.8 copy-start
  374.6 7.8 %copy-start.10 = (s32[512,2]{0,1:T(2,128)S(1)}, s32[512,2]{0,1:T(2,128)}, u32[]{:S(2)}) copy-start(s32[512,2]{0,1:T(2,128)} %param.28) | copy-start | bytes 12292
  374.6 8.0 %copy-start.11 = (f32[512,2]{0,1:T(2,128)S(1)}, f32[512,2]{0,1:T(2,128)}, u32[]{:S(2)}) copy-start(f32[512,2]{0,1:T(2,128)} %param.30) | copy-start | bytes 12292
  374.6 8.1 %copy-start.14 = (f32[512]{0:T(512)S(1)}, f32[512]{0:T(512)}, u32[]{:S(2)}) copy-start(f32[512]{0:T(512)} %param.29) | copy-start | bytes 6148
  374.6 49.4 %all-to-all-start.2 = ((bf16[1024,32,2,24]{0,3,2,1:T(8,128)(2,1)}), bf16[1024,32,2,24]{0,3,2,1:T(8,128)(2,1)S(1)}, u32[]{:S(2)}, u32[]{:S(2)}) async-start(bf16[1024,32,2,24]{0,3,2,1:T(8,128)(2,1)} %copy.182), calls=%async_computation.3 | async-start | bytes 6291456 | tf_op jit(solution)/shard_map/all_to_all | solution.py:196
Sparse Core Ops, SparseCore 0:
  106.1 42.5 all-gather.11
  152.7 84.1 all-gather.13
Sparse Core Ops, SparseCore 1:
  275.5 65.3 all-gather.9
  343.8 89.0 reduce-scatter.1
